TPU v7x, 32 devices: a whole 2x2x4 slice. The times are simulated.
32 devices in a mesh: rep: 2 (over x), fs: 8 (over z, y), tp: 2 (over core).
Axes of the slice: x: 2, y: 2, z: 4, core: 2. Of those that a mesh axis runs over, the one named last changes fastest.
Arguments:
- x_early: bfloat16 [1792, 2048], P(('rep', 'fs')), may hold values from -6 to 6
- x_late: bfloat16 [1792, 2048], P(('rep', 'fs')), may hold values from -6 to 6
- grad_out: bfloat16 [1792, 2048], P(('rep', 'fs')), may hold values from -6 to 6
- w_gate: bfloat16 [2048, 3072], P('fs', 'tp'), may hold values from -0.125 to 0.125
- w_up: bfloat16 [2048, 3072], P('fs', 'tp'), may hold values from -0.125 to 0.125
- w_down: bfloat16 [3072, 2048], P('tp', 'fs'), may hold values from -0.109375 to 0.109375
- gate_sum: float32 [2048, 3072], P('fs', 'tp'), may hold values from -80 to 80
- up_sum: float32 [2048, 3072], P('fs', 'tp'), may hold values from -80 to 80
- down_sum: float32 [3072, 2048], P('tp', 'fs'), may hold values from -80 to 80
Outputs:
- out_late: bfloat16 [1792, 2048], P(('rep', 'fs'))
- grad_in: bfloat16 [1792, 2048], P(('rep', 'fs'))
- new_gate_sum: float32 [2048, 3072], P('fs', 'tp')
- new_up_sum: float32 [2048, 3072], P('fs', 'tp')
- new_down_sum: float32 [3072, 2048], P('tp', 'fs')
All inputs are finite; a program needn't handle non-finite values.
Results may differ from a plain program's by a relative error of at most 0.018.
Values may be sent and summed in bfloat16 or wider, within the bound.
A program may use at most 128 MiB of HBM per device.

v0:
```python
import jax
import jax.numpy as jnp
from jax import lax
from jax.sharding import PartitionSpec as P

epsilon = 1e-06


def contract_rows(left, right):
    return lax.dot_general(
        left, right, (((0,), (0,)), ((), ())), preferred_element_type=jnp.float32
    )


def contract_cols(left, right):
    return lax.dot_general(
        left, right, (((1,), (1,)), ((), ())), preferred_element_type=jnp.float32
    )


def shards(x_early, x_late, grad_out, w_gate, w_up, w_down, gate_sum, up_sum, down_sum):
    gate_full, up_full, down_full = (
        lax.all_gather(w_gate, "fs", axis=0, tiled=True),
        lax.all_gather(w_up, "fs", axis=0, tiled=True),
        lax.all_gather(w_down, "fs", axis=1, tiled=True),
    )
    batch_rows = x_early.shape[0]
    stacked = jnp.concatenate([x_early, x_late], axis=0).astype(jnp.float32)
    row_scale = lax.rsqrt(jnp.mean(stacked * stacked, axis=-1, keepdims=True) + epsilon)
    normed = (stacked * row_scale).astype(jnp.bfloat16)
    gate_pre = jnp.dot(normed, gate_full, preferred_element_type=jnp.float32)
    up_pre = jnp.dot(normed, up_full, preferred_element_type=jnp.float32)
    gate_sig = jax.nn.sigmoid(gate_pre)
    hidden = (gate_pre * gate_sig * up_pre).astype(jnp.bfloat16)
    late_part = jnp.dot(hidden[batch_rows:], down_full, preferred_element_type=jnp.float32).astype(
        jnp.bfloat16
    )
    branch = lax.psum(late_part, "tp").astype(jnp.float32)
    out_late = (stacked[batch_rows:] + 0.5 * branch).astype(jnp.bfloat16)
    early_gate = gate_pre[:batch_rows]
    early_upper = up_pre[:batch_rows]
    early_sig = gate_sig[:batch_rows]
    early_hidden = hidden[:batch_rows]
    early_normed = normed[:batch_rows]
    early_scale = row_scale[:batch_rows]
    grad_hidden = 0.5 * contract_cols(grad_out, down_full)
    grad_gate_in = (
        grad_hidden * early_upper * early_sig * (1.0 + early_gate * (1.0 - early_sig))
    ).astype(jnp.bfloat16)
    grad_up_in = (grad_hidden * early_gate * early_sig).astype(jnp.bfloat16)
    normed_part = contract_cols(grad_gate_in, gate_full) + contract_cols(grad_up_in, up_full)
    grad_normed = lax.psum(normed_part.astype(jnp.bfloat16), "tp").astype(jnp.float32)
    unit_rows = stacked[:batch_rows] * early_scale
    inner = jnp.mean(grad_normed * unit_rows, axis=-1, keepdims=True)
    grad_in = (
        grad_out.astype(jnp.float32) + early_scale * (grad_normed - unit_rows * inner)
    ).astype(jnp.bfloat16)
    normed_cols, out_cols = (
        lax.all_to_all(early_normed, "fs", split_axis=1, concat_axis=0, tiled=True),
        lax.all_to_all(grad_out, "fs", split_axis=1, concat_axis=0, tiled=True),
    )
    gate_delta = contract_rows(normed_cols, lax.all_gather(grad_gate_in, "fs", axis=0, tiled=True))
    up_delta = contract_rows(normed_cols, lax.all_gather(grad_up_in, "fs", axis=0, tiled=True))
    down_half = contract_rows(lax.all_gather(early_hidden, "fs", axis=0, tiled=True), out_cols)
    down_delta = 0.5 * down_half
    gate_delta, up_delta, down_delta = (
        lax.psum(gate_delta.astype(jnp.bfloat16), "rep").astype(jnp.float32),
        lax.psum(up_delta.astype(jnp.bfloat16), "rep").astype(jnp.float32),
        lax.psum(down_delta.astype(jnp.bfloat16), "rep").astype(jnp.float32),
    )
    return (out_late, grad_in, gate_sum + gate_delta, up_sum + up_delta, down_sum + down_delta)


def solution(mesh):
    placed = (
        P(("rep", "fs"), None),
        P(("rep", "fs"), None),
        P(("rep", "fs"), None),
        P("fs", "tp"),
        P("fs", "tp"),
        P("tp", "fs"),
        P("fs", "tp"),
        P("fs", "tp"),
        P("tp", "fs"),
    )
    return jax.shard_map(
        shards,
        mesh=mesh,
        in_specs=placed,
        out_specs=(
            P(("rep", "fs"), None),
            P(("rep", "fs"), None),
            P("fs", "tp"),
            P("fs", "tp"),
            P("tp", "fs"),
        ),
        check_vma=False,
    )
```

profile of v0, /device:TPU:0, one launch (start us, length us, event | category | flops | bytes accessed | tf_op | source)
XLA Modules:
  0.0 608.1 jit_solution(10017036902288530399)
XLA Ops:
  7.2 0.0 copy-start.1
  7.2 0.0 copy-start.2
  7.2 0.0 all-gather.9.cloned.1.call-start
  7.2 0.7 all-gather.9.cloned.1.call-update
  7.9 0.0 all-gather.7.cloned.1.call-start
  8.0 0.7 all-gather.7.cloned.1.call-update
  8.7 0.0 all-gather.11.cloned.1.call-start
  8.7 0.7 all-gather.11.cloned.1.call-update
  9.4 0.0 all-gather.13.cloned.1.call-start
  9.4 0.0 copy-done.1
  9.5 0.0 copy-done.2
  9.5 0.3 multiply_reduce_fusion
  9.7 0.2 multiply_convert_fusion
  10.0 0.0 copy-start.4
  10.0 101.6 %all-gather.9.cloned.1.call-done = bf16[2048,1536]{1,0:T(8,128)(2,1)} async-done(((bf16[256,1536]{1,0:T(8,128)(2,1)}), bf16[2048,1536]{1,0:T(8,128)(2,1)}) %all-gather.9.cloned.1.call-update) | async-done | bytes 6291472 | tf_op jit(solution)/shard_map/all_gather | solution.py:24
  111.6 5.4 fusion.11
  117.1 0.0 copy-start
  117.1 93.6 %all-gather.7.cloned.1.call-done = bf16[2048,1536]{1,0:T(8,128)(2,1)} async-done(((bf16[256,1536]{1,0:T(8,128)(2,1)}), bf16[2048,1536]{1,0:T(8,128)(2,1)}) %all-gather.7.cloned.1.call-update) | async-done | bytes 6291472 | tf_op jit(solution)/shard_map/all_gather | solution.py:23
  210.7 0.0 copy-done.4
  210.7 6.5 %add_divide_fusion = (f32[224,1536]{1,0:T(8,128)}, bf16[224,1536]{1,0:T(8,128)(2,1)}, f32[224,1536]{1,0:T(8,128)}) fusion(f32[224,1536]{1,0:T(8,128)} %fusion.11, bf16[224,2048]{1,0:T(8,128)(2,1)S(1)} %multiply_convert_fusion, bf16[2048,1536]{1,0:T(8,128)(2,1)} %all-gather.7.cloned.1.call-done), kind=kOutput, calls=%fused_computation.14 | convolution fusion | flops 1411350528 | bytes 12025856 | tf_op jit(solution)/shard_map/dot_general | solution.py:31
  217.3 93.2 %all-gather.11.cloned.1.call-done = bf16[1536,2048]{1,0:T(8,128)(2,1)} async-done(((bf16[1536,256]{1,0:T(8,128)(2,1)}), bf16[1536,2048]{1,0:T(8,128)(2,1)}) %all-gather.11.cloned.1.call-update) | async-done | bytes 6291472 | tf_op jit(solution)/shard_map/all_gather | solution.py:25
  310.5 0.0 copy-done
  310.5 6.4 %multiply_convert_fusion.2 = (bf16[112,1536]{1,0:T(8,128)(2,1)}, bf16[112,1536]{1,0:T(8,128)(2,1)}) fusion(f32[224,1536]{1,0:T(8,128)} %get-tuple-element.16, f32[224,1536]{1,0:T(8,128)} %get-tuple-element.14, f32[224,1536]{1,0:T(8,128)} %fusion.11, bf16[112,2048]{1,0:T(8,128)(2,1)S(1)} %copy-done, bf16[1536,2048]{1,0:T(8,128)(2,1)} %all-gather.11.cloned.1.call-done), kind=kOutput, calls=%fused_computation.29 | convolution fusion | flops 706535424 | bytes 9502720 | tf_op jit(solution)/shard_map/dot_general | solution.py:16
  316.9 0.0 all-gather.13.cloned.1.call-update
  316.9 0.0 all-gather.15.cloned.1.call-start
  317.0 0.5 all-gather.15.cloned.1.call-update
  317.5 0.0 all-gather.17.cloned.1.call-start
  317.5 0.0 slice-start
  317.6 1.9 slice.44
  319.5 0.0 all-gather.17.cloned.1.call-update
  319.5 1.0 slice.43
  320.5 0.8 copy.24
  321.3 4.1 all-to-all-start
  325.5 0.8 copy.23
  326.3 0.0 slice-start.1
  326.3 5.1 fusion.12
  331.4 0.0 slice-done
  331.4 0.0 slice-done.1
  331.4 0.0 copy-done.3
  331.4 2.8 fusion.1
  334.2 13.9 %all-to-all-done = bf16[112,8,256]{2,0,1:T(8,128)(2,1)} async-done(((bf16[112,8,256]{2,0,1:T(8,128)(2,1)}), bf16[112,8,256]{2,0,1:T(8,128)(2,1)}, u32[]{:S(2)}, u32[]{:S(2)}) %all-to-all-start) | async-done | bytes 458784 | tf_op jit(solution)/shard_map/all_to_all | solution.py:59
  348.1 3.5 all-to-all-start.1
  351.6 0.0 all-reduce.5.cloned.1.call-start
  351.7 5.1 convolution_convert_fusion.2
  356.8 0.0 all-reduce.5.cloned.1.call-update
  356.8 0.2 all-reduce.7.cloned.1.call-start
  357.0 30.3 %all-gather.13.cloned.1.call-done = bf16[896,1536]{1,0:T(8,128)(2,1)} async-done(((bf16[112,1536]{1,0:T(8,128)(2,1)}), bf16[896,1536]{1,0:T(8,128)(2,1)}) %all-gather.13.cloned.1.call-update) | async-done | bytes 2752528 | tf_op jit(solution)/shard_map/all_gather | solution.py:62
  387.3 3.8 convolution_convert_fusion.1
  391.1 53.3 %all-gather.15.cloned.1.call-done = bf16[896,1536]{1,0:T(8,128)(2,1)} async-done(((bf16[112,1536]{1,0:T(8,128)(2,1)}), bf16[896,1536]{1,0:T(8,128)(2,1)}) %all-gather.15.cloned.1.call-update) | async-done | bytes 2752528 | tf_op jit(solution)/shard_map/all_gather | solution.py:63
  444.5 3.8 convolution_convert_fusion
  448.3 0.0 all-to-all-done.1
  448.3 52.9 %all-gather.17.cloned.1.call-done = bf16[896,1536]{1,0:T(8,128)(2,1)} async-done(((bf16[112,1536]{1,0:T(8,128)(2,1)}), bf16[896,1536]{1,0:T(8,128)(2,1)}) %all-gather.17.cloned.1.call-update) | async-done | bytes 2752528 | tf_op jit(solution)/shard_map/all_gather | solution.py:64
  501.1 3.7 fusion
  504.8 0.0 all-reduce.7.cloned.1.call-update
  504.9 0.2 maximum_convert_fusion
  505.1 16.9 %all-reduce.5.cloned.1.call-done = (bf16[112,2048]{1,0:T(8,128)(2,1)}, bf16[112,2048]{1,0:T(8,128)(2,1)}) async-done(((bf16[112,2048]{1,0:T(8,128)(2,1)}, bf16[112,2048]{1,0:T(8,128)(2,1)}), (bf16[112,2048]{1,0:T(8,128)(2,1)}, bf16[112,2048]{1,0:T(8,128)(2,1)})) %all-reduce.5.cloned.1.call-update) | async-done | bytes 917520 | tf_op jit(solution)/shard_map/psum | solution.py:38
  522.0 1.3 fusion.2
  523.3 2.5 fusion.5
  525.8 69.1 %all-reduce.7.cloned.1.call-done = (bf16[256,1536]{1,0:T(8,128)(2,1)}, bf16[256,1536]{1,0:T(8,128)(2,1)}, bf16[1536,256]{1,0:T(8,128)(2,1)}) async-done(((bf16[256,1536]{1,0:T(8,128)(2,1)}, bf16[256,1536]{1,0:T(8,128)(2,1)}, bf16[1536,256]{1,0:T(8,128)(2,1)}), (bf16[256,1536]{1,0:T(8,128)(2,1)}, bf16[256,1536]{1,0:T(8,128)(2,1)}, bf16[1536,256]{1,0:T(8,128)(2,1)})) %all-reduce.7.cloned.1.call-update) | async-done | bytes 2359312 | tf_op jit(solution)/shard_map/psum | solution.py:67
  594.9 3.1 convert_add_fusion
  598.0 0.0 copy-done.5
  598.0 0.0 copy-done.6
  598.0 0.0 copy-done.7
  598.0 3.3 convert_add_fusion.1
  (8 shorter events, 0.0 us)
Async XLA Ops:
  7.2 2.3 copy-start.1
  7.2 2.3 copy-start.2
  7.2 104.4 %all-gather.9.cloned.1.call-start = ((), (), s32[]{:S(2)}) async-start(), calls=%async_computation.3 | async-start | bytes 7077888 | tf_op jit(solution)/shard_map/all_gather | solution.py:24
  7.9 202.8 %all-gather.7.cloned.1.call-start = ((), (), s32[]{:S(2)}) async-start(), calls=%async_computation.2 | async-start | bytes 7077888 | tf_op jit(solution)/shard_map/all_gather | solution.py:23
  8.7 301.8 %all-gather.11.cloned.1.call-start = ((), (), s32[]{:S(2)}) async-start(), calls=%async_computation.4 | async-start | bytes 7077888 | tf_op jit(solution)/shard_map/all_gather | solution.py:25
  9.4 377.9 %all-gather.13.cloned.1.call-start = ((), (), s32[]{:S(2)}) async-start(), calls=%async_computation.5 | async-start | bytes 3096576 | tf_op jit(solution)/shard_map/all_gather | solution.py:62
  10.0 200.7 %copy-start.4 = (bf16[224,2048]{1,0:T(8,128)(2,1)}, bf16[224,2048]{1,0:T(8,128)(2,1)S(1)}, u32[]{:S(2)}) copy-start(bf16[224,2048]{1,0:T(8,128)(2,1)S(1)} %multiply_convert_fusion) | copy-start | bytes 2752516
  117.1 193.4 %copy-start = (bf16[112,2048]{1,0:T(8,128)(2,1)S(1)}, bf16[112,2048]{1,0:T(8,128)(2,1)}, u32[]{:S(2)}) copy-start(bf16[112,2048]{1,0:T(8,128)(2,1)} %param.11) | copy-start | bytes 1376260
  316.9 127.5 %all-gather.15.cloned.1.call-start = ((), (), s32[]{:S(2)}) async-start(), calls=%async_computation.6 | async-start | bytes 3096576 | tf_op jit(solution)/shard_map/all_gather | solution.py:63
  317.5 183.6 %all-gather.17.cloned.1.call-start = ((), (), s32[]{:S(2)}) async-start(), calls=%async_computation.7 | async-start | bytes 3096576 | tf_op jit(solution)/shard_map/all_gather | solution.py:64
  317.5 13.8 %slice-start = ((s8[6291456]{0:T(1024)(128)(4,1)}), s8[2097152]{0:T(1024)(128)(4,1)S(1)}, s32[]{:S(2)}) async-start(s8[6291456]{0:T(1024)(128)(4,1)} %bitcast.31), calls=%async_computation.10 | async-start | bytes 4194304
  321.3 26.8 %all-to-all-start = ((bf16[112,8,256]{2,0,1:T(8,128)(2,1)}), bf16[112,8,256]{2,0,1:T(8,128)(2,1)}, u32[]{:S(2)}, u32[]{:S(2)}) async-start(bf16[112,8,256]{2,0,1:T(8,128)(2,1)} %bitcast.35), calls=%async_computation | async-start | bytes 917504 | tf_op jit(solution)/shard_map/all_to_all | solution.py:59
  326.3 5.1 slice-start.1
  326.3 5.1 copy-start.3
  348.1 100.1 %all-to-all-start.1 = ((bf16[112,8,256]{2,0,1:T(8,128)(2,1)}), bf16[112,8,256]{2,0,1:T(8,128)(2,1)S(1)}, u32[]{:S(2)}, u32[]{:S(2)}) async-start(bf16[112,8,256]{2,0,1:T(8,128)(2,1)} %bitcast.34), calls=%async_computation.1 | async-start | bytes 917504 | tf_op jit(solution)/shard_map/all_to_all | solution.py:60
  351.6 170.3 %all-reduce.5.cloned.1.call-start = ((), (), s32[]{:S(2)}) async-start(), calls=%async_computation.8 | async-start | bytes 1835008 | tf_op jit(solution)/shard_map/psum | solution.py:38
  356.8 238.1 %all-reduce.7.cloned.1.call-start = ((), (), s32[]{:S(2)}) async-start(), calls=%async_computation.9 | async-start | bytes 4718592 | tf_op jit(solution)/shard_map/psum | solution.py:67
  594.9 3.1 copy-start.5
  594.9 3.1 copy-start.6
  594.9 3.1 copy-start.7
Sparse Core Ops, SparseCore 0:
  10.2 101.4 all-gather.8
  113.8 96.8 all-gather.6
  212.8 97.6 all-gather.10
  317.0 70.2 all-gather.12
  389.3 55.0 all-gather.14
  446.5 54.5 all-gather.16
  504.1 17.8 all-reduce.4
  525.0 69.9 all-reduce.6
where the time goes:
time: 609 us; the launch traced here: 608 us
  waiting for transfers between devices  528 us (87%)
  matrix products  42.7 us (7%)
  between operations  14.3 us (2%)
  other arithmetic  10.9 us (2%)
  starting transfers between devices  8.12 us (1%)
    all_gather x1, waiting for transfers between devices, shards(): lax.all_gather(w_up, 'fs', axis=0, tiled=True)  102 us
    all_gather x1, waiting for transfers between devices, shards(): lax.all_gather(w_gate, 'fs', axis=0, tiled=True)  93.6 us
    all_gather x1, waiting for transfers between devices, shards(): lax.all_gather(w_down, 'fs', axis=1, tiled=True)  93.2 us
    psum x1, waiting for transfers between devices, shards(): lax.psum(gate_delta.astype(jnp.bfloat16), 'rep').astype(jnp.float32)  69.1 us
    all_gather x1, waiting for transfers between devices, shards(): lax.all_gather(grad_up_in, 'fs', axis=0, tiled=True)  53.3 us
    all_gather x1, waiting for transfers between devices, shards(): lax.all_gather(early_hidden, 'fs', axis=0, tiled=True)  52.9 us
    all_gather x1, waiting for transfers between devices, shards(): lax.all_gather(grad_gate_in, 'fs', axis=0, tiled=True)  30.3 us
    psum x1, waiting for transfers between devices, shards(): branch = lax.psum(late_part, 'tp').astype(jnp.float32)  16.9 us
  transfers between devices with their start and end apart: 10, of which 9 were waited for; matrix products, arithmetic and copies ran while one was open for 7% of the time, Pallas kernels for 0%

commit v1 on v0

--- a/solution.py
+++ b/solution.py
@@ -4,6 +4,10 @@
 from jax.sharding import PartitionSpec as P
 
 epsilon = 1e-06
+
+
+def serve_counts(state, net_axis):
+    return lax.all_gather(state, net_axis).sum(axis=0)
 
 
 def contract_rows(left, right):
@@ -64,7 +68,7 @@
     down_half = contract_rows(lax.all_gather(early_hidden, "fs", axis=0, tiled=True), out_cols)
     down_delta = 0.5 * down_half
     gate_delta, up_delta, down_delta = (
-        lax.psum(gate_delta.astype(jnp.bfloat16), "rep").astype(jnp.float32),
+        serve_counts(gate_delta.astype(jnp.bfloat16), "rep").astype(jnp.float32),
         lax.psum(up_delta.astype(jnp.bfloat16), "rep").astype(jnp.float32),
         lax.psum(down_delta.astype(jnp.bfloat16), "rep").astype(jnp.float32),
     )

time: 609 us -> 612 us (level)
    all_gather x1, waiting for transfers between devices: 53.3 us -> 20.4 us  [shards(): lax.all_gather(grad_up_in, 'fs', axis=0, tiled=True)]
    all_gather x1, waiting for transfers between devices: 30.3 us -> 58.1 us  [shards(): lax.all_gather(grad_gate_in, 'fs', axis=0, tiled=True)]
    all_gather x0 -> x1, waiting for transfers between devices: none -> 24.9 us  [serve_counts(): return lax.all_gather(state, net_axis).sum(axis=0)]
    psum x1, waiting for transfers between devices: 69.1 us -> 47.9 us  [shards(): lax.psum(up_delta.astype(jnp.bfloat16), 'rep').astype(jnp.float32)]
  transfers between devices with their start and end apart: 10 -> 11, of which waited for: 9 -> 10; matrix products, arithmetic and copies ran while one was open for 7% -> 8% of each run, Pallas kernels for 0% -> 0%
where the time goes in v1:
time: 612 us; the launch traced here: 611 us
  waiting for transfers between devices  534 us (87%)
  matrix products  42.2 us (7%)
  between operations  14 us (2%)
  other arithmetic  10.8 us (2%)
  starting transfers between devices  7.81 us (1%)
    all_gather x1, waiting for transfers between devices, shards(): lax.all_gather(w_up, 'fs', axis=0, tiled=True)  102 us
    all_gather x1, waiting for transfers between devices, shards(): lax.all_gather(w_gate, 'fs', axis=0, tiled=True)  93.6 us
    all_gather x1, waiting for transfers between devices, shards(): lax.all_gather(w_down, 'fs', axis=1, tiled=True)  93.4 us
    all_gather x1, waiting for transfers between devices, shards(): lax.all_gather(grad_gate_in, 'fs', axis=0, tiled=True)  58.1 us
    all_gather x1, waiting for transfers between devices, shards(): lax.all_gather(early_hidden, 'fs', axis=0, tiled=True)  54.5 us
    psum x1, waiting for transfers between devices, shards(): lax.psum(up_delta.astype(jnp.bfloat16), 'rep').astype(jnp.float32)  47.9 us
    all_gather x1, waiting for transfers between devices, serve_counts(): return lax.all_gather(state, net_axis).sum(axis=0)  24.9 us
    all_gather x1, waiting for transfers between devices, shards(): lax.all_gather(grad_up_in, 'fs', axis=0, tiled=True)  20.4 us
  transfers between devices with their start and end apart: 11, of which 10 were waited for; matrix products, arithmetic and copies ran while one was open for 8% of the time, Pallas kernels for 0%

profile of v1, /device:TPU:0, one launch (start us, length us, event | category | flops | bytes accessed | tf_op | source)
XLA Modules:
  0.0 611.1 jit_solution(16582507389899302037)
XLA Ops:
  7.2 0.0 copy-start.1
  7.2 0.0 copy-start.2
  7.2 0.0 all-gather.11.cloned.1.call-start
  7.2 0.7 all-gather.11.cloned.1.call-update
  7.9 0.0 all-gather.9.cloned.1.call-start
  8.0 0.7 all-gather.9.cloned.1.call-update
  8.7 0.0 all-gather.13.cloned.1.call-start
  8.7 0.7 all-gather.13.cloned.1.call-update
  9.4 0.0 all-gather.17.cloned.1.call-start
  9.4 0.0 copy-done.1
  9.5 0.0 copy-done.2
  9.5 0.3 multiply_reduce_fusion
  9.7 0.2 multiply_convert_fusion
  10.0 0.0 copy-start.5
  10.0 101.6 %all-gather.11.cloned.1.call-done = bf16[2048,1536]{1,0:T(8,128)(2,1)} async-done(((bf16[256,1536]{1,0:T(8,128)(2,1)}), bf16[2048,1536]{1,0:T(8,128)(2,1)}) %all-gather.11.cloned.1.call-update) | async-done | bytes 6291472 | tf_op jit(solution)/shard_map/all_gather | solution.py:28
  111.6 5.4 fusion.11
  117.1 93.6 %all-gather.9.cloned.1.call-done = bf16[2048,1536]{1,0:T(8,128)(2,1)} async-done(((bf16[256,1536]{1,0:T(8,128)(2,1)}), bf16[2048,1536]{1,0:T(8,128)(2,1)}) %all-gather.9.cloned.1.call-update) | async-done | bytes 6291472 | tf_op jit(solution)/shard_map/all_gather | solution.py:27
  210.7 0.0 copy-done.5
  210.7 6.3 %add_divide_fusion = (f32[224,1536]{1,0:T(8,128)}, bf16[224,1536]{1,0:T(8,128)(2,1)S(1)}, f32[224,1536]{1,0:T(8,128)}) fusion(f32[224,1536]{1,0:T(8,128)} %fusion.11, bf16[224,2048]{1,0:T(8,128)(2,1)S(1)} %multiply_convert_fusion, bf16[2048,1536]{1,0:T(8,128)(2,1)} %all-gather.9.cloned.1.call-done), kind=kOutput, calls=%fused_computation.14 | convolution fusion | flops 1411350528 | bytes 12025856 | tf_op jit(solution)/shard_map/dot_general | solution.py:35
  217.0 93.4 %all-gather.13.cloned.1.call-done = bf16[1536,2048]{1,0:T(8,128)(2,1)} async-done(((bf16[1536,256]{1,0:T(8,128)(2,1)}), bf16[1536,2048]{1,0:T(8,128)(2,1)}) %all-gather.13.cloned.1.call-update) | async-done | bytes 6291472 | tf_op jit(solution)/shard_map/all_gather | solution.py:29
  310.5 0.0 copy-done
  310.5 6.4 %multiply_convert_fusion.2 = (bf16[112,1536]{1,0:T(8,128)(2,1)}, bf16[112,1536]{1,0:T(8,128)(2,1)}) fusion(f32[224,1536]{1,0:T(8,128)} %get-tuple-element.15, f32[224,1536]{1,0:T(8,128)} %get-tuple-element.13, f32[224,1536]{1,0:T(8,128)} %fusion.11, bf16[112,2048]{1,0:T(8,128)(2,1)S(1)} %copy-done, bf16[1536,2048]{1,0:T(8,128)(2,1)} %all-gather.13.cloned.1.call-done), kind=kOutput, calls=%fused_computation.29 | convolution fusion | flops 706535424 | bytes 9502720 | tf_op jit(solution)/shard_map/dot_general | solution.py:20
  316.9 0.0 all-gather.17.cloned.1.call-update
  316.9 0.0 all-gather.19.cloned.1.call-start
  317.0 0.0 copy-done.10
  317.0 0.8 slice.44
  317.7 0.0 all-gather.19.cloned.1.call-update
  317.8 0.0 all-reduce.5.cloned.1.call-start
  317.8 0.0 slice-start
  317.8 4.8 convolution_convert_fusion.2
  322.7 5.2 fusion.12
  327.9 2.8 fusion.1
  330.7 0.0 all-reduce.5.cloned.1.call-update
  330.8 0.0 all-gather.15.cloned.1.call-start
  330.8 0.7 all-gather.15.cloned.1.call-update
  331.5 0.2 slice-done.2
  331.8 0.8 copy.24
  332.6 3.5 all-to-all-start
  336.0 0.8 copy.23
  336.8 19.6 %all-to-all-done = bf16[112,8,256]{2,0,1:T(8,128)(2,1)S(1)} async-done(((bf16[112,8,256]{2,0,1:T(8,128)(2,1)}), bf16[112,8,256]{2,0,1:T(8,128)(2,1)S(1)}, u32[]{:S(2)}, u32[]{:S(2)}) %all-to-all-start) | async-done | bytes 458784 | tf_op jit(solution)/shard_map/all_to_all | solution.py:63
  356.5 3.8 all-to-all-start.1
  360.3 0.0 all-reduce.7.cloned.1.call-start
  360.3 20.4 %all-gather.17.cloned.1.call-done = bf16[896,1536]{1,0:T(8,128)(2,1)} async-done(((bf16[112,1536]{1,0:T(8,128)(2,1)}), bf16[896,1536]{1,0:T(8,128)(2,1)}) %all-gather.17.cloned.1.call-update) | async-done | bytes 2752528 | tf_op jit(solution)/shard_map/all_gather | solution.py:67
  380.7 3.7 convolution_convert_fusion
  384.4 0.0 all-to-all-done.1
  384.4 54.5 %all-gather.19.cloned.1.call-done = bf16[896,1536]{1,0:T(8,128)(2,1)} async-done(((bf16[112,1536]{1,0:T(8,128)(2,1)}), bf16[896,1536]{1,0:T(8,128)(2,1)}) %all-gather.19.cloned.1.call-update) | async-done | bytes 2752528 | tf_op jit(solution)/shard_map/all_gather | solution.py:68
  438.9 3.7 fusion
  442.6 0.0 all-reduce.7.cloned.1.call-update
  442.6 0.2 all-gather.21.cloned.1.call-start
  442.9 0.2 maximum_convert_fusion
  443.1 16.5 %all-reduce.5.cloned.1.call-done = (bf16[112,2048]{1,0:T(8,128)(2,1)}, bf16[112,2048]{1,0:T(8,128)(2,1)}) async-done(((bf16[112,2048]{1,0:T(8,128)(2,1)}, bf16[112,2048]{1,0:T(8,128)(2,1)}), (bf16[112,2048]{1,0:T(8,128)(2,1)}, bf16[112,2048]{1,0:T(8,128)(2,1)})) %all-reduce.5.cloned.1.call-update) | async-done | bytes 917520 | tf_op jit(solution)/shard_map/psum | solution.py:42
  459.6 1.3 fusion.2
  461.0 58.1 %all-gather.15.cloned.1.call-done = bf16[896,1536]{1,0:T(8,128)(2,1)} async-done(((bf16[112,1536]{1,0:T(8,128)(2,1)}), bf16[896,1536]{1,0:T(8,128)(2,1)}) %all-gather.15.cloned.1.call-update) | async-done | bytes 2752528 | tf_op jit(solution)/shard_map/all_gather | solution.py:66
  519.0 3.8 convolution_convert_fusion.1
  522.8 0.0 all-gather.21.cloned.1.call-update
  522.9 0.0 copy-done.6
  522.9 0.0 copy-done.11
  522.9 1.4 fusion.5
  524.2 47.9 %all-reduce.7.cloned.1.call-done = (bf16[256,1536]{1,0:T(8,128)(2,1)}, bf16[1536,256]{1,0:T(8,128)(2,1)}) async-done(((bf16[256,1536]{1,0:T(8,128)(2,1)}, bf16[1536,256]{1,0:T(8,128)(2,1)}), (bf16[256,1536]{1,0:T(8,128)(2,1)}, bf16[1536,256]{1,0:T(8,128)(2,1)})) %all-reduce.7.cloned.1.call-update) | async-done | bytes 1572880 | tf_op jit(solution)/shard_map/psum | solution.py:72
  572.1 3.1 convert_add_fusion
  575.2 1.4 convert_add_fusion.1
  576.6 24.9 %all-gather.21.cloned.1.call-done = bf16[512,1536]{1,0:T(8,128)(2,1)} async-done(((bf16[256,1536]{1,0:T(8,128)(2,1)}), bf16[512,1536]{1,0:T(8,128)(2,1)}) %all-gather.21.cloned.1.call-update) | async-done | bytes 1572880 | tf_op jit(solution)/shard_map/all_gather | solution.py:10
  601.5 1.7 reduce_sum.32
  603.2 1.3 convert_add_fusion.2
  (22 shorter events, 0.0 us)
Async XLA Ops:
  7.2 2.3 copy-start.1
  7.2 2.3 copy-start.2
  7.2 104.4 %all-gather.11.cloned.1.call-start = ((), (), s32[]{:S(2)}) async-start(), calls=%async_computation.3 | async-start | bytes 7077888 | tf_op jit(solution)/shard_map/all_gather | solution.py:28
  7.9 202.8 %all-gather.9.cloned.1.call-start = ((), (), s32[]{:S(2)}) async-start(), calls=%async_computation.2 | async-start | bytes 7077888 | tf_op jit(solution)/shard_map/all_gather | solution.py:27
  8.7 301.8 %all-gather.13.cloned.1.call-start = ((), (), s32[]{:S(2)}) async-start(), calls=%async_computation.4 | async-start | bytes 7077888 | tf_op jit(solution)/shard_map/all_gather | solution.py:29
  9.4 371.3 %all-gather.17.cloned.1.call-start = ((), (), s32[]{:S(2)}) async-start(), calls=%async_computation.6 | async-start | bytes 3096576 | tf_op jit(solution)/shard_map/all_gather | solution.py:67
  10.0 200.7 %copy-start.5 = (bf16[224,2048]{1,0:T(8,128)(2,1)}, bf16[224,2048]{1,0:T(8,128)(2,1)S(1)}, u32[]{:S(2)}) copy-start(bf16[224,2048]{1,0:T(8,128)(2,1)S(1)} %multiply_convert_fusion) | copy-start | bytes 2752516
  117.1 193.4 %copy-start = (bf16[112,2048]{1,0:T(8,128)(2,1)S(1)}, bf16[112,2048]{1,0:T(8,128)(2,1)}, u32[]{:S(2)}) copy-start(bf16[112,2048]{1,0:T(8,128)(2,1)} %param.11) | copy-start | bytes 1376260
  217.0 100.0 %copy-start.10 = (bf16[224,1536]{1,0:T(8,128)(2,1)}, bf16[224,1536]{1,0:T(8,128)(2,1)S(1)}, u32[]{:S(2)}) copy-start(bf16[224,1536]{1,0:T(8,128)(2,1)S(1)} %get-tuple-element.14) | copy-start | bytes 2064388
  316.9 122.0 %all-gather.19.cloned.1.call-start = ((), (), s32[]{:S(2)}) async-start(), calls=%async_computation.7 | async-start | bytes 3096576 | tf_op jit(solution)/shard_map/all_gather | solution.py:68
  317.8 141.8 %all-reduce.5.cloned.1.call-start = ((), (), s32[]{:S(2)}) async-start(), calls=%async_computation.9 | async-start | bytes 1835008 | tf_op jit(solution)/shard_map/psum | solution.py:42
  317.8 10.1 %slice-start = ((s8[6291456]{0:T(1024)(128)(4,1)}), s8[2097152]{0:T(1024)(128)(4,1)S(1)}, s32[]{:S(2)}) async-start(s8[6291456]{0:T(1024)(128)(4,1)} %bitcast.32), calls=%async_computation.11 | async-start | bytes 4194304
  322.6 5.2 slice-start.1
  322.7 5.2 copy-start.4
  330.7 1.0 slice-start.2
  330.8 188.3 %all-gather.15.cloned.1.call-start = ((), (), s32[]{:S(2)}) async-start(), calls=%async_computation.5 | async-start | bytes 3096576 | tf_op jit(solution)/shard_map/all_gather | solution.py:66
  332.6 23.9 %all-to-all-start = ((bf16[112,8,256]{2,0,1:T(8,128)(2,1)}), bf16[112,8,256]{2,0,1:T(8,128)(2,1)S(1)}, u32[]{:S(2)}, u32[]{:S(2)}) async-start(bf16[112,8,256]{2,0,1:T(8,128)(2,1)} %bitcast.31), calls=%async_computation | async-start | bytes 917504 | tf_op jit(solution)/shard_map/all_to_all | solution.py:63
  356.5 27.9 %copy-start.3 = (bf16[112,8,256]{2,0,1:T(8,128)(2,1)}, bf16[112,8,256]{2,0,1:T(8,128)(2,1)S(1)}, u32[]{:S(2)}) copy-start(bf16[112,8,256]{2,0,1:T(8,128)(2,1)S(1)} %all-to-all-done) | copy-start | bytes 1376260
  356.5 27.9 %all-to-all-start.1 = ((bf16[112,8,256]{2,0,1:T(8,128)(2,1)}), bf16[112,8,256]{2,0,1:T(8,128)(2,1)S(1)}, u32[]{:S(2)}, u32[]{:S(2)}) async-start(bf16[112,8,256]{2,0,1:T(8,128)(2,1)} %bitcast.30), calls=%async_computation.1 | async-start | bytes 917504 | tf_op jit(solution)/shard_map/all_to_all | solution.py:64
  360.3 211.9 %all-reduce.7.cloned.1.call-start = ((), (), s32[]{:S(2)}) async-start(), calls=%async_computation.10 | async-start | bytes 3145728 | tf_op jit(solution)/shard_map/psum | solution.py:72
  442.6 158.8 %all-gather.21.cloned.1.call-start = ((), (), s32[]{:S(2)}) async-start(), calls=%async_computation.8 | async-start | bytes 2359296 | tf_op jit(solution)/shard_map/all_gather | solution.py:10
  460.9 61.9 %copy-start.6 = (bf16[112,2048]{1,0:T(8,128)(2,1)S(1)}, bf16[112,2048]{1,0:T(8,128)(2,1)}, u32[]{:S(2)}) copy-start(bf16[112,2048]{1,0:T(8,128)(2,1)} %get-tuple-element.6) | copy-start | bytes 1376260
  460.9 61.9 %copy-start.11 = (bf16[112,2048]{1,0:T(8,128)(2,1)S(1)}, bf16[112,2048]{1,0:T(8,128)(2,1)}, u32[]{:S(2)}) copy-start(bf16[112,2048]{1,0:T(8,128)(2,1)} %get-tuple-element.5) | copy-start | bytes 1376260
  572.1 3.1 copy-start.7
  572.1 3.1 copy-start.9
  576.6 26.6 %copy-start.8 = (f32[256,1536]{1,0:T(8,128)S(1)}, f32[256,1536]{1,0:T(8,128)}, u32[]{:S(2)}) copy-start(f32[256,1536]{1,0:T(8,128)} %param.15) | copy-start | bytes 4718596
Sparse Core Ops, SparseCore 0:
  10.2 101.4 all-gather.10
  113.8 96.8 all-gather.8
  212.8 97.6 all-gather.12
  317.0 63.6 all-gather.16
  383.3 55.5 all-gather.18
  441.7 17.8 all-reduce.4
  461.8 57.1 all-gather.14
  522.0 50.1 all-reduce.6
  574.3 27.1 all-gather.20
